TPU v7x, 32 devices: a whole 2x2x4 slice. The times are simulated.
32 devices in a mesh: ep: 8 (over z, core), tp: 4 (over y, x).
Axes of the slice: x: 2, y: 2, z: 4, core: 2. Of those that a mesh axis runs over, the one named last changes fastest.
Arguments:
- compressed_query: bfloat16 [1024, 1536], P('ep'), may hold values from -6 to 6
- compressed_key_value: bfloat16 [1024, 512], P('ep'), may hold values from -6 to 6
- rotary_key: bfloat16 [1024, 32], P('ep'), may hold values from -600 to 600
- query_norm_scale: float32 [1536], replicated, may hold values from 0.1 to 1.9
- context_norm_scale: float32 [512], replicated, may hold values from 0.1 to 1.9
- query_plain_weight: bfloat16 [1536, 1024], P(None, 'tp'), may hold values from -0.375 to 0.375
- query_rotary_weight: bfloat16 [1536, 512], P(None, 'tp'), may hold values from -0.375 to 0.375
- key_up_weight: bfloat16 [512, 1024], P(None, 'tp'), may hold values from -0.25 to 0.25
- value_up_weight: bfloat16 [512, 1024], P(None, 'tp'), may hold values from -0.25 to 0.25
- output_weight: bfloat16 [1024, 2048], P(None, 'tp'), may hold values from -0.75 to 0.75
- mixture_input: bfloat16 [1024, 2048], P('ep'), may hold values from -6 to 6
- mixture_gain: float32 [2048], replicated, may hold values from 0.1 to 1.9
- routes: int32 [1024, 2], P('ep'), may hold values from 0 to 7, all different within a row; in each aligned block of 128 rows (0 to 127, 128 to 255, ...) at most 48 rows name the same one
- route_weight: float32 [1024, 2], P('ep'), may hold values from 0.2 to 2
- expert_gate: bfloat16 [8, 2048, 4096], P('ep', None, 'tp'), may hold values from -0.125 to 0.125
- expert_up: bfloat16 [8, 2048, 4096], P('ep', None, 'tp'), may hold values from -0.125 to 0.125
- expert_down: bfloat16 [8, 4096, 2048], P('ep', None, 'tp'), may hold values from -0.09375 to 0.09375
- shared_gate: bfloat16 [2048, 512], P(None, 'tp'), may hold values from -0.125 to 0.125
- shared_up: bfloat16 [2048, 512], P(None, 'tp'), may hold values from -0.125 to 0.125
- shared_down: bfloat16 [512, 2048], P(None, 'tp'), may hold values from -0.25 to 0.25
Outputs:
- attended: bfloat16 [1024, 2048], P('ep', 'tp')
- combined: bfloat16 [1024, 2048], P('ep', 'tp')
Inputs may be any that keep to these rules, and one draw needn't show every extreme that they name: `routes`: in the rows of each index of ep, no expert is named more than 48 times, a bound that some block reaches there.
All inputs are finite; a program needn't handle non-finite values.
Results may differ from a plain program's by a relative error of at most 0.012.
The roundings to bfloat16 on the way count: a program that leaves them out, or rounds other values in their place, can miss the bound.
Values may be sent and summed in bfloat16 or wider, within the bound.
A program may use at most 64 MiB of HBM per device.

v0:
```python
import math

import jax
import jax.numpy as jnp
from jax import lax
from jax.sharding import PartitionSpec as P

PLAIN_HEAD_SIZE = 64
ROTARY_SIZE = 32
VALUE_HEAD_SIZE = 64
TOPK = 2


def normed_rows(values, scaling):
    floats = values.astype(jnp.float32)
    return floats * lax.rsqrt(jnp.mean(floats * floats, axis=-1, keepdims=True) + 1e-06) * scaling


def rotary_tables(positions):
    inverse = 1.0 / 10000.0 ** (jnp.arange(0, ROTARY_SIZE, 2, dtype=jnp.float32) / ROTARY_SIZE)
    angles = positions.astype(jnp.float32)[:, None] * inverse[None, :]
    return (jnp.cos(angles), jnp.sin(angles))


def rotate(vectors, cosine, sine_part):
    half_width = vectors.shape[-1] // 2
    front_half = vectors[..., :half_width]
    back_half = vectors[..., half_width:]
    return jnp.concatenate(
        [front_half * cosine - back_half * sine_part, front_half * sine_part + back_half * cosine],
        axis=-1,
    )


def fold_blocks(carry_state, members, handle):
    length = members[0].shape[0]
    block_rows = math.gcd(length, 2048)

    def advance(block_index, carried):
        sliced = tuple(
            (
                lax.dynamic_slice_in_dim(member, block_index * block_rows, block_rows, 0)
                for member in members
            )
        )
        return handle(carried, sliced, block_index * block_rows)

    return lax.fori_loop(0, length // block_rows, advance, carry_state)


def per_device(
    compressed_query,
    compressed_key_value,
    rotary_key,
    query_norm_scale,
    context_norm_scale,
    query_plain_weight,
    query_rotary_weight,
    key_up_weight,
    value_up_weight,
    output_weight,
    mixture_input,
    mixture_gain,
    routes,
    route_weight,
    expert_gate,
    expert_up,
    expert_down,
    shared_gate,
    shared_up,
    shared_down,
):
    tokens = compressed_query.shape[0]
    heads_here = query_plain_weight.shape[1] // PLAIN_HEAD_SIZE
    offset = lax.axis_index("ep") * tokens
    cosine, sine_part = rotary_tables(offset + jnp.arange(tokens, dtype=jnp.int32))
    compressed = normed_rows(compressed_query, query_norm_scale).astype(jnp.bfloat16)
    query_nope = jnp.dot(compressed, query_plain_weight, preferred_element_type=jnp.float32)
    query_nope = query_nope.astype(jnp.bfloat16).reshape(tokens, heads_here, PLAIN_HEAD_SIZE)
    query_turn = jnp.dot(compressed, query_rotary_weight, preferred_element_type=jnp.float32)
    query_turn = query_turn.reshape(tokens, heads_here, ROTARY_SIZE)
    query_rot = rotate(query_turn, cosine[:, None, :], sine_part[:, None, :])
    context = normed_rows(compressed_key_value, context_norm_scale).astype(jnp.bfloat16)
    scale = (PLAIN_HEAD_SIZE + ROTARY_SIZE) ** (-0.5)
    start_state = (
        jnp.full((heads_here, tokens), -1e30, jnp.float32),
        jnp.zeros((heads_here, tokens), jnp.float32),
        jnp.zeros((heads_here, tokens, VALUE_HEAD_SIZE), jnp.float32),
    )

    def attend(carry_state, sliced, first_row):
        key_rows, value_rows, raw_turn = sliced
        count = raw_turn.shape[0]
        key_cos, key_sin = rotary_tables(first_row + jnp.arange(count, dtype=jnp.int32))
        turned = rotate(raw_turn.astype(jnp.float32), key_cos, key_sin)
        running_max, running_total, running_sum = carry_state
        key_heads = key_rows.reshape(count, heads_here, PLAIN_HEAD_SIZE)
        value_heads = value_rows.reshape(count, heads_here, VALUE_HEAD_SIZE)
        scores = (
            jnp.einsum("qhe,khe->hqk", query_nope, key_heads, preferred_element_type=jnp.float32)
            + jnp.einsum("qhr,kr->hqk", query_rot, turned, precision=lax.Precision.HIGHEST)
        ) * scale
        new_max = jnp.maximum(running_max, jnp.max(scores, axis=-1))
        factor = jnp.exp(running_max - new_max)
        weights = jnp.exp(scores - new_max[..., None])
        running_total = running_total * factor + jnp.sum(weights, axis=-1)
        running_sum = running_sum * factor[..., None] + jnp.einsum(
            "hqk,khe->hqe",
            weights.astype(jnp.bfloat16),
            value_heads,
            preferred_element_type=jnp.float32,
        )
        return (new_max, running_total, running_sum)

    def expand(carry_state, sliced, first_row):
        latent_rows, raw_turn = sliced
        key_rows = jnp.dot(latent_rows, key_up_weight, preferred_element_type=jnp.float32).astype(
            jnp.bfloat16
        )
        value_rows = jnp.dot(
            latent_rows, value_up_weight, preferred_element_type=jnp.float32
        ).astype(jnp.bfloat16)
        return attend(carry_state, (key_rows, value_rows, raw_turn), first_row)

    final_state = fold_blocks(
        start_state,
        (
            lax.all_gather(context, "ep", axis=0, tiled=True),
            lax.all_gather(rotary_key, "ep", axis=0, tiled=True),
        ),
        expand,
    )
    heads_out = final_state[2] / final_state[1][..., None]
    heads_out = (
        heads_out.transpose(1, 0, 2)
        .reshape(tokens, heads_here * VALUE_HEAD_SIZE)
        .astype(jnp.bfloat16)
    )
    all_heads = lax.all_gather(heads_out, "tp", axis=1, tiled=True)
    attended = jnp.dot(all_heads, output_weight, preferred_element_type=jnp.float32).astype(
        jnp.bfloat16
    )
    floats = mixture_input.astype(jnp.float32)
    centred = floats - jnp.mean(floats, axis=-1, keepdims=True)
    normed = (
        centred
        * lax.rsqrt(jnp.mean(centred * centred, axis=-1, keepdims=True) + 1e-05)
        * mixture_gain
    ).astype(jnp.bfloat16)
    experts = lax.axis_size("ep")
    rows_here = mixture_input.shape[0]
    model_width = normed.shape[1]
    capacity = rows_here * TOPK * 3 // (2 * experts)
    flat_routes = routes.reshape(-1)
    one_hot = (flat_routes[:, None] == jnp.arange(experts, dtype=jnp.int32)[None, :]).astype(
        jnp.int32
    )
    ranks = jnp.sum(one_hot * (jnp.cumsum(one_hot, axis=0) - 1), axis=1)
    slots = flat_routes * capacity + ranks
    owners = jnp.full((experts * capacity,), rows_here, jnp.int32)
    owners = owners.at[slots].set(jnp.arange(rows_here * TOPK, dtype=jnp.int32) // TOPK)
    padded = jnp.concatenate([normed, jnp.zeros((1, model_width), jnp.bfloat16)], axis=0)
    outgoing = padded[owners].reshape(experts, capacity, model_width)
    arrived = lax.all_to_all(outgoing, "ep", split_axis=0, concat_axis=0, tiled=True).reshape(
        experts * capacity, model_width
    )
    hidden = (
        jax.nn.silu(jnp.dot(arrived, expert_gate[0], preferred_element_type=jnp.float32))
        * jnp.dot(arrived, expert_up[0], preferred_element_type=jnp.float32)
    ).astype(jnp.bfloat16)
    shared_hidden = (
        jax.nn.silu(jnp.dot(normed, shared_gate, preferred_element_type=jnp.float32))
        * jnp.dot(normed, shared_up, preferred_element_type=jnp.float32)
    ).astype(jnp.bfloat16)
    all_hidden, all_shared = (
        lax.all_gather(hidden, "tp", axis=1, tiled=True),
        lax.all_gather(shared_hidden, "tp", axis=1, tiled=True),
    )
    expert_rows = jnp.dot(all_hidden, expert_down[0], preferred_element_type=jnp.float32).astype(
        jnp.bfloat16
    )
    features = expert_rows.shape[1]
    returned = lax.all_to_all(
        expert_rows.reshape(experts, capacity, features),
        "ep",
        split_axis=0,
        concat_axis=0,
        tiled=True,
    )
    picked = returned.reshape(experts * capacity, features)[slots]
    picked = picked.astype(jnp.float32).reshape(rows_here, TOPK, features)
    routed = jnp.sum(picked * route_weight[:, :, None], axis=1)
    combined = (
        jnp.dot(all_shared, shared_down, preferred_element_type=jnp.float32) + routed
    ).astype(jnp.bfloat16)
    return (attended, combined)


def solution(mesh):
    in_specs = (
        P("ep", None),
        P("ep", None),
        P("ep", None),
        P(),
        P(),
        P(None, "tp"),
        P(None, "tp"),
        P(None, "tp"),
        P(None, "tp"),
        P(None, "tp"),
        P("ep", None),
        P(),
        P("ep", None),
        P("ep", None),
        P("ep", None, "tp"),
        P("ep", None, "tp"),
        P("ep", None, "tp"),
        P(None, "tp"),
        P(None, "tp"),
        P(None, "tp"),
    )
    out_specs = (P("ep", "tp"), P("ep", "tp"))
    return jax.shard_map(
        per_device, mesh=mesh, in_specs=in_specs, out_specs=out_specs, check_vma=False
    )
```

profile of v0, /device:TPU:0, one launch (start us, length us, event | category | flops | bytes accessed | tf_op | source)
XLA Modules:
  0.0 154.8 jit_solution(1504360362727506415)
XLA Ops:
  7.2 0.9 copy.28
  8.3 0.7 broadcast_multiply_fusion
  9.0 0.6 reduce-window.6
  10.2 1.4 scatter_custom_fusion
  11.7 1.2 convert_reduce_fusion
  12.9 1.3 fusion.21
  14.2 1.4 fusion.23
  15.7 3.1 %gather_fusion = bf16[384,2048]{1,0:T(8,128)(2,1)} fusion(bf16[129,2048]{1,0:T(8,128)(2,1)S(1)} %concatenate.12, s32[1024]{0:T(1024)S(1)} %pad_clamp_fusion.1), kind=kCustom, calls=%fused_computation | custom fusion | bytes 3147264 | tf_op jit(solution)/shard_map/gather | solution.py:163
  18.8 6.5 %all-to-all-start = ((bf16[8,48,2048]{2,1,0:T(8,128)(2,1)}), bf16[8,48,2048]{2,1,0:T(8,128)(2,1)S(1)}, u32[]{:S(2)}, u32[]{:S(2)}) async-start(bf16[8,48,2048]{2,1,0:T(8,128)(2,1)} %bitcast.14), calls=%async_computation | async-start | bytes 3145728 | tf_op jit(solution)/shard_map/all_to_all | solution.py:164
  25.5 0.8 fusion.31
  26.3 45.2 %all-to-all-done = bf16[8,48,2048]{2,1,0:T(8,128)(2,1)S(1)} async-done(((bf16[8,48,2048]{2,1,0:T(8,128)(2,1)}), bf16[8,48,2048]{2,1,0:T(8,128)(2,1)S(1)}, u32[]{:S(2)}, u32[]{:S(2)}) %all-to-all-start) | async-done | bytes 1572896 | tf_op jit(solution)/shard_map/all_to_all | solution.py:164
  71.5 4.1 %fusion.4 = f32[384,1024]{1,0:T(8,128)S(1)} fusion(bf16[384,2048]{1,0:T(8,128)(2,1)S(1)} %bitcast.76, bf16[1,2048,1024]{2,1,0:T(8,128)(2,1)} %param.34), kind=kOutput, calls=%fused_computation.7 | convolution fusion | flops 1610612736 | bytes 7340032 | tf_op jit(solution)/shard_map/dot_general | solution.py:168
  75.7 2.9 %multiply_convert_fusion = bf16[384,1024]{1,0:T(8,128)(2,1)} fusion(f32[384,1024]{1,0:T(8,128)S(1)} %fusion.4, bf16[384,2048]{1,0:T(8,128)(2,1)S(1)} %bitcast.77, bf16[1,2048,1024]{2,1,0:T(8,128)(2,1)S(1)} %copy-done.13), kind=kOutput, calls=%fused_computation.14 | convolution fusion | flops 1612972032 | bytes 8126464 | tf_op jit(solution)/shard_map/dot_general | solution.py:169
  78.8 1.6 %convolution_convert_fusion.3 = bf16[128,256]{1,0:T(8,128)(2,1)S(1)} fusion(bf16[1536,256]{1,0:T(8,128)(2,1)} %param.25, bf16[128,1536]{1,0:T(8,128)(2,1)S(1)} %copy-done.6, f32[1536]{0:T(1024)S(1)} %copy-done.16, f32[128]{0:T(128)S(1)} %add_rsqrt_fusion.2), kind=kOutput, calls=%fused_computation.28 | convolution fusion | flops 101482496 | bytes 1251840 | tf_op jit(solution)/shard_map/dot_general | solution.py:78
  80.5 12.8 %all_gather.16 = bf16[1024,32]{0,1:T(8,128)(2,1)S(1)} all-gather(bf16[128,32]{0,1:T(8,128)(2,1)S(1)} %copy-done.10), channel_id=1, replica_groups=mesh['ep'=8,'tp'=4] {'ep'}, dimensions={0}, use_global_device_ids=true | all-gather | bytes 73728 | tf_op jit(solution)/shard_map/all_gather | solution.py:129
  93.4 0.7 copy.30
  94.7 9.3 %all_gather.18 = bf16[128,512]{1,0:T(8,128)(2,1)} all-gather(bf16[128,128]{1,0:T(8,128)(2,1)S(1)} %fusion.20), channel_id=1, replica_groups=mesh['ep'=8,'tp'=4] {'tp'}, dimensions={1}, use_global_device_ids=true | all-gather | bytes 163840 | tf_op jit(solution)/shard_map/all_gather | solution.py:177
  104.1 0.6 pad_clamp_fusion
  105.6 1.7 %convolution_convert_fusion.1 = bf16[1024,256]{0,1:T(8,128)(2,1)S(1)} fusion(bf16[1024,512]{1,0:T(8,128)(2,1)} %all-gather.3.cloned.1.call-done, bf16[512,256]{1,0:T(8,128)(2,1)S(1)} %copy-done.7), kind=kOutput, calls=%fused_computation.18 | convolution fusion | flops 268697600 | bytes 1835008 | tf_op jit(solution)/shard_map/while/body/eval_jaxpr/dot_general | solution.py:117
  107.8 2.0 %fusion.51 = (f32[4,128]{1,0:T(4,128)S(1)}, f32[4,128,1024]{2,1,0:T(8,128)S(1)}) fusion(f32[4,128,1024]{2,1,0:T(8,128)S(1)} %fusion.52, f32[128,4,16]{0,2,1:T(8,128)S(1)} %get-tuple-element.27, f32[128,4,16]{0,2,1:T(8,128)S(1)} %get-tuple-element.26, f32[1024,16]{0,1:T(8,128)S(1)} %get-tuple-element.25, f32[1024,16]{0,1:T(8,128)S(1)} %get-tuple-element.24), kind=kOutput, calls=%fused_computation.94 | convolution fusion | flops 202948096 | bytes 4392960 | tf_op jit(solution)/shard_map/while/body/eval_jaxpr/qhr,kr->hqk/dot_general | solution.py:101
  110.3 0.7 copy-done.1
  111.1 1.3 convolution_convert_fusion
  112.3 9.5 %all-gather.5.cloned.1.call-done = bf16[384,4096]{1,0:T(8,128)(2,1)} async-done(((bf16[384,1024]{1,0:T(8,128)(2,1)}), bf16[384,4096]{1,0:T(8,128)(2,1)}) %all-gather.5.cloned.1.call-update) | async-done | bytes 3145744 | tf_op jit(solution)/shard_map/all_gather | solution.py:176
  121.8 5.7 %fusion.11 = bf16[384,512]{1,0:T(8,128)(2,1)} fusion(bf16[384,4096]{1,0:T(8,128)(2,1)} %all-gather.5.cloned.1.call-done, bf16[1,4096,512]{2,1,0:T(8,128)(2,1)} %param.36), kind=kOutput, calls=%fused_computation.19 | convolution fusion | flops 1610809344 | bytes 7733248 | tf_op jit(solution)/shard_map/dot_general | solution.py:179
  127.5 4.6 %all-to-all-start.1 = ((bf16[8,48,512]{2,1,0:T(8,128)(2,1)}), bf16[8,48,512]{2,1,0:T(8,128)(2,1)S(1)}, u32[]{:S(2)}, u32[]{:S(2)}) async-start(bf16[8,48,512]{2,1,0:T(8,128)(2,1)} %bitcast.78), calls=%async_computation.1 | async-start | bytes 786432 | tf_op jit(solution)/shard_map/all_to_all | solution.py:183
  132.1 1.6 %fusion.19 = bf16[128,4,64]{0,2,1:T(8,128)(2,1)S(1)} fusion(bf16[1024,4,64]{0,2,1:T(8,128)(2,1)} %bitcast.74, f32[4,128,1024]{2,1,0:T(8,128)S(1)} %get-tuple-element.44, f32[4,128]{1,0:T(4,128)S(1)} %get-tuple-element.29, f32[128,4]{0,1:T(4,128)S(1)} %bitcast_add_fusion.1, f32[128,4]{0,1:T(4,128)S(1)} %get-tuple-element.28), kind=kOutput, calls=%fused_computation.29 | convolution fusion | flops 68255744 | bytes 2693120 | tf_op jit(solution)/shard_map/while/body/eval_jaxpr/hqk,khe->hqe/dot_general | solution.py:107
  133.8 8.9 %all_gather.17 = bf16[128,1024]{0,1:T(8,128)(2,1)S(1)} all-gather(bf16[128,256]{0,1:T(8,128)(2,1)S(1)} %bitcast.79), channel_id=1, replica_groups=mesh['ep'=8,'tp'=4] {'tp'}, dimensions={1}, use_global_device_ids=true | all-gather | bytes 327680 | tf_op jit(solution)/shard_map/all_gather | solution.py:139
  142.7 1.0 convolution_convert_fusion.2
  143.7 1.0 all-to-all-done.1
  144.6 1.3 gather_fusion.1
  146.3 0.7 multiply_reduce_fusion
  147.0 0.9 fusion.16
  (74 shorter events, 4.4 us)
Async XLA Ops:
  7.2 135.5 %copy-start = (bf16[1024,512]{1,0:T(8,128)(2,1)S(1)}, bf16[1024,512]{1,0:T(8,128)(2,1)}, u32[]{:S(2)}) copy-start(bf16[1024,512]{1,0:T(8,128)(2,1)} %param.29) | copy-start | bytes 3145732
  18.8 6.5 %copy-start.4 = (bf16[128,512]{1,0:T(8,128)(2,1)S(1)}, bf16[128,512]{1,0:T(8,128)(2,1)}, u32[]{:S(2)}) copy-start(bf16[128,512]{1,0:T(8,128)(2,1)} %param.21) | copy-start | bytes 393220
  18.8 6.7 %copy-start.11 = (f32[512]{0:T(512)S(1)}, f32[512]{0:T(512)}, u32[]{:S(2)}) copy-start(f32[512]{0:T(512)} %param.24) | copy-start | bytes 6148
  18.8 52.7 %all-to-all-start = ((bf16[8,48,2048]{2,1,0:T(8,128)(2,1)}), bf16[8,48,2048]{2,1,0:T(8,128)(2,1)S(1)}, u32[]{:S(2)}, u32[]{:S(2)}) async-start(bf16[8,48,2048]{2,1,0:T(8,128)(2,1)} %bitcast.14), calls=%async_computation | async-start | bytes 3145728 | tf_op jit(solution)/shard_map/all_to_all | solution.py:164
  25.3 80.2 %all-gather.3.cloned.1.call-start = ((), (), s32[]{:S(2)}) async-start(), calls=%async_computation.2 | async-start | bytes 1179648 | tf_op jit(solution)/shard_map/all_gather | solution.py:128
  26.3 95.6 %all-gather.5.cloned.1.call-start = ((), (), s32[]{:S(2)}) async-start(), calls=%async_computation.3 | async-start | bytes 3932160 | tf_op jit(solution)/shard_map/all_gather | solution.py:176
  71.5 4.2 %copy-start.13 = (bf16[1,2048,1024]{2,1,0:T(8,128)(2,1)S(1)}, bf16[1,2048,1024]{2,1,0:T(8,128)(2,1)}, u32[]{:S(2)}) copy-start(bf16[1,2048,1024]{2,1,0:T(8,128)(2,1)} %param.35) | copy-start | bytes 12582916
  75.7 2.9 %copy-start.6 = (bf16[128,1536]{1,0:T(8,128)(2,1)S(1)}, bf16[128,1536]{1,0:T(8,128)(2,1)}, u32[]{:S(2)}) copy-start(bf16[128,1536]{1,0:T(8,128)(2,1)} %param.20) | copy-start | bytes 1179652
  75.7 3.1 %copy-start.16 = (f32[1536]{0:T(1024)S(1)}, f32[1536]{0:T(1024)}, u32[]{:S(2)}) copy-start(f32[1536]{0:T(1024)} %param.23) | copy-start | bytes 18436
  78.6 1.9 %copy-start.10 = (bf16[128,32]{0,1:T(8,128)(2,1)S(1)}, bf16[128,32]{0,1:T(8,128)(2,1)}, u32[]{:S(2)}) copy-start(bf16[128,32]{0,1:T(8,128)(2,1)} %param.22) | copy-start | bytes 24580
  78.6 14.8 %copy-start.12 = (f32[128,2]{0,1:T(2,128)S(1)}, f32[128,2]{0,1:T(2,128)}, u32[]{:S(2)}) copy-start(f32[128,2]{0,1:T(2,128)} %param.33) | copy-start | bytes 3076
  78.6 15.5 %copy-start.2 = (bf16[2048,128]{1,0:T(8,128)(2,1)S(1)}, bf16[2048,128]{1,0:T(8,128)(2,1)}, u32[]{:S(2)}) copy-start(bf16[2048,128]{1,0:T(8,128)(2,1)} %param.37) | copy-start | bytes 1572868
  78.6 15.8 %copy-start.14 = (bf16[2048,128]{1,0:T(8,128)(2,1)S(1)}, bf16[2048,128]{1,0:T(8,128)(2,1)}, u32[]{:S(2)}) copy-start(bf16[2048,128]{1,0:T(8,128)(2,1)} %param.38) | copy-start | bytes 1572868
  80.5 25.0 %copy-start.7 = (bf16[512,256]{1,0:T(8,128)(2,1)S(1)}, bf16[512,256]{1,0:T(8,128)(2,1)}, u32[]{:S(2)}) copy-start(bf16[512,256]{1,0:T(8,128)(2,1)} %param.27) | copy-start | bytes 786436
  94.1 10.7 %copy-start.15 = (bf16[1536,128]{1,0:T(8,128)(2,1)S(1)}, bf16[1536,128]{1,0:T(8,128)(2,1)}, u32[]{:S(2)}) copy-start(bf16[1536,128]{1,0:T(8,128)(2,1)} %param.26) | copy-start | bytes 1179652
  109.8 1.2 copy-start.1
  109.8 1.3 copy-start.8
  127.5 17.1 %all-to-all-start.1 = ((bf16[8,48,512]{2,1,0:T(8,128)(2,1)}), bf16[8,48,512]{2,1,0:T(8,128)(2,1)S(1)}, u32[]{:S(2)}, u32[]{:S(2)}) async-start(bf16[8,48,512]{2,1,0:T(8,128)(2,1)} %bitcast.78), calls=%async_computation.1 | async-start | bytes 786432 | tf_op jit(solution)/shard_map/all_to_all | solution.py:183
  142.7 3.6 %copy-start.9 = (f32[128,2]{1,0:T(8,128)S(1)}, f32[128,2]{1,0:T(8,128)}, u32[]{:S(2)}) copy-start(f32[128,2]{1,0:T(8,128)} %copy.30) | copy-start | bytes 3076
  143.7 3.3 %copy-start.3 = (bf16[512,512]{1,0:T(8,128)(2,1)S(1)}, bf16[512,512]{1,0:T(8,128)(2,1)}, u32[]{:S(2)}) copy-start(bf16[512,512]{1,0:T(8,128)(2,1)} %param.39) | copy-start | bytes 1572868
  143.7 3.3 %copy-start.5 = (bf16[128,512]{1,0:T(8,128)(2,1)S(1)}, bf16[128,512]{1,0:T(8,128)(2,1)}, u32[]{:S(2)}) copy-start(bf16[128,512]{1,0:T(8,128)(2,1)} %all_gather.18) | copy-start | bytes 393220
Sparse Core Ops, SparseCore 0:
  28.3 37.9 all-gather.2
  78.7 43.0 all-gather.4
where the time goes:
time: 155 us
  waiting for transfers between devices  55.7 us (36%)
  blocking collectives  31.1 us (20%)
  matrix products  24.2 us (16%)
  between operations  14.4 us (9%)
  starting transfers between devices  11.2 us (7%)
  local copies, waits for them, and re-layouts  9.52 us (6%)
  other arithmetic  8.67 us (6%)
    all_to_all x1, waiting for transfers between devices, per_device(): lax.all_to_all(outgoing, 'ep', split_axis=0, concat_axis=0, tiled=True)  45.2 us
    all_gather x1, blocking collectives, per_device(): lax.all_gather(rotary_key, 'ep', axis=0, tiled=True)  12.8 us
    all_gather x1, waiting for transfers between devices, per_device(): lax.all_gather(hidden, 'tp', axis=1, tiled=True)  9.5 us
    all_gather x1, blocking collectives, per_device(): lax.all_gather(shared_hidden, 'tp', axis=1, tiled=True)  9.33 us
    all_gather x1, blocking collectives, per_device(): all_heads = lax.all_gather(heads_out, 'tp', axis=1, tiled=True)  8.93 us
    all_to_all x1, starting transfers between devices, per_device(): lax.all_to_all(outgoing, 'ep', split_axis=0, concat_axis=0, tiled=True)  6.49 us
    dot_general x1, matrix products, per_device(): jnp.dot(all_hidden, expert_down[0], preferred_element_type=jnp.float32)  5.67 us
    all_to_all x1, starting transfers between devices, per_device(): lax.all_to_all(expert_rows.reshape(experts, capacity, features), 'ep', sp...  4.62 us
  transfers between devices with their start and end apart: 4, of which 3 were waited for; matrix products, arithmetic and copies ran while one was open for 14% of the time, Pallas kernels for 0%

commit v1 on v0

v1 whole, which is shorter than its diff:
```python
import functools

import jax
import jax.numpy as jnp
from jax import lax
from jax.experimental import pallas as pl
from jax.experimental.pallas import tpu as pltpu
from jax.sharding import PartitionSpec as P

PLAIN = 64
ROT = 32
VALUE = 64
TOPK = 2
F32 = jnp.float32
BF16 = jnp.bfloat16
MESH = pl.DeviceIdType.MESH


def dot(a, b):
    return jnp.dot(a, b, preferred_element_type=F32)


def dot_t(a, b):
    return lax.dot_general(a, b, (((1,), (1,)), ((), ())), preferred_element_type=F32)


def tdot(a, b):
    return lax.dot_general(a, b, (((0,), (0,)), ((), ())), preferred_element_type=F32)


def body(
    E, T, NC,
    cq, ckv, rkt, qscale, cscale, mx, mgain, routes, rweight, cosq, sinq, cosk, sink,
    qp_h, qr_h, ku_h, vu_h, ow_h, gate_h, up_h, down_h, sg_h, su_h, sd_h,
    attended, combined,
    qp, qr, ku, vu, ow, gate, up, down, sg, su, sd,
    normed, outgoing, arr, kv, rk, shared, heads, hidden, rows_out, returned,
    wsem,
    sa, ra, sb, rb, skv, rkv, srk, rrk, ssh, rsh, shd, rhd, sh, rh, sd2, rd2, sr, rr,
):
    ep = lax.axis_index("ep")
    tp = lax.axis_index("tp")
    tx, ty = lax.rem(tp, 2), tp // 2
    xp = ty * 2 + (1 - tx)
    yp = (1 - ty) * 2 + tx
    dg = (1 - ty) * 2 + (1 - tx)
    square = T == 4
    tpeers = (xp, yp, dg) if square else [lax.rem(tp + d, T) for d in range(1, T)]
    eps = [lax.rem(ep + d, E) for d in range(1, E)]
    eps_back = [lax.rem(ep - d + E, E) for d in range(1, E)]
    tokens = mx.shape[0]
    cp = outgoing.shape[1]
    width = outgoing.shape[2]
    slots = E * cp
    ff = gate.shape[1]

    loads = []
    pairs = (
        (sg_h, sg), (su_h, su), (ku_h, ku), (vu_h, vu), (qp_h, qp), (qr_h, qr),
        (gate_h, gate), (up_h, up), (down_h, down), (ow_h, ow), (sd_h, sd),
    )
    for i, (src, dst) in enumerate(pairs):
        load = pltpu.make_async_copy(src, dst, wsem.at[i])
        load.start()
        loads.append(load)
    l_sg, l_su, l_ku, l_vu, l_qp, l_qr, l_gate, l_up, l_down, l_ow, l_sd = loads

    barrier = pltpu.get_barrier_semaphore()
    for e in eps:
        pl.semaphore_signal(barrier, inc=1, device_id=(e, tp), device_id_type=MESH)
    for q in tpeers:
        pl.semaphore_signal(barrier, inc=1, device_id=(ep, q), device_id_type=MESH)

    def remote(src, dst, send, recv, e, q):
        return pltpu.make_async_remote_copy(
            src_ref=src, dst_ref=dst, send_sem=send, recv_sem=recv,
            device_id=(e, q), device_id_type=MESH,
        )

    floats = mx[...].astype(F32)
    centred = floats - jnp.mean(floats, axis=-1, keepdims=True)
    normed[...] = (
        centred
        * lax.rsqrt(jnp.mean(centred * centred, axis=-1, keepdims=True) + 1e-05)
        * mgain[...]
    ).astype(BF16)

    experts = lax.broadcasted_iota(jnp.int32, (E, tokens), 0)
    r0, r1 = routes[0:1, :], routes[1:2, :]
    hit0 = (experts == r0).astype(F32)
    hit1 = (experts == r1).astype(F32)
    before = (
        lax.broadcasted_iota(jnp.int32, (tokens, tokens), 0)
        < lax.broadcasted_iota(jnp.int32, (tokens, tokens), 1)
    ).astype(F32).astype(BF16)
    ranks = dot((hit0 + hit1).astype(BF16), before)
    slot0 = r0 * cp + jnp.sum(hit0 * ranks, axis=0, keepdims=True).astype(jnp.int32)
    slot1 = r1 * cp + jnp.sum(hit1 * ranks, axis=0, keepdims=True).astype(jnp.int32)
    places = lax.broadcasted_iota(jnp.int32, (slots, tokens), 0)
    pick0 = (places == slot0).astype(F32)
    pick1 = (places == slot1).astype(F32)
    mine = normed[:, pl.ds(pl.multiple_of(tp * width, width), width)]
    outgoing[...] = dot((pick0 + pick1).astype(BF16), mine).astype(BF16).reshape(E, cp, width)
    arr[tp, ep] = outgoing[ep]

    pl.semaphore_wait(barrier, (E - 1) + (T - 1))

    sends = []
    for e in eps:
        c = remote(outgoing.at[e], arr.at[tp, ep], sa.at[e], ra.at[ep], e, tp)
        c.start()
        sends.append(c)

    def forward(s):
        for q in tpeers:
            c = remote(arr.at[tp, s], arr.at[tp, s], sb.at[q, s], rb.at[tp, s], ep, q)
            c.start()
            sends.append(c)

    forward(ep)

    def rms(values, scaling):
        v = values.astype(F32)
        return (v * lax.rsqrt(jnp.mean(v * v, axis=-1, keepdims=True) + 1e-06) * scaling).astype(BF16)

    context = rms(ckv[...], cscale[...])
    kw = ku.shape[1]
    l_ku.wait()
    kv[ep, :, 0:kw] = dot(context, ku[...]).astype(BF16)
    l_vu.wait()
    kv[ep, :, kw:] = dot(context, vu[...]).astype(BF16)
    rk[ep] = rkt[...]
    for e in eps:
        c = remote(kv.at[ep], kv.at[ep], skv.at[e], rkv.at[ep], e, tp)
        c.start()
        sends.append(c)
        c = remote(rk.at[ep], rk.at[ep], srk.at[e], rrk.at[ep], e, tp)
        c.start()
        sends.append(c)

    l_sg.wait()
    l_su.wait()
    g = dot(normed[...], sg[...])
    shared[tp] = (g / (1.0 + jnp.exp(-g)) * dot(normed[...], su[...])).astype(BF16)
    for q in tpeers:
        c = remote(shared.at[tp], shared.at[tp], ssh.at[q], rsh.at[tp], ep, q)
        c.start()
        sends.append(c)

    for s in eps_back:
        remote(arr.at[tp, s], arr.at[tp, s], sa.at[s], ra.at[s], s, tp).wait_recv()
        forward(s)

    compressed = rms(cq[...], qscale[...])
    l_qp.wait()
    query = dot(compressed, qp[...]).astype(BF16)
    l_qr.wait()
    turn = dot(compressed, qr[...])
    tw = turn.shape[1]
    lane = lax.broadcasted_iota(jnp.int32, turn.shape, 1)
    if tw % 128 == 0:
        swapped = jnp.where(
            lax.rem(lane, ROT) < ROT // 2,
            pltpu.roll(turn, tw - ROT // 2, 1),
            pltpu.roll(turn, ROT // 2, 1),
        )
    else:
        cuts = [turn[:, i:i + ROT // 2] for i in range(0, tw, ROT // 2)]
        swapped = jnp.concatenate([cuts[i + 1 - 2 * (i % 2)] for i in range(len(cuts))], axis=1)
    query_rot = turn * cosq[...] + swapped * sinq[...]

    l_gate.wait()
    l_up.wait()
    per = E // NC
    tile, out_tile = min(256, ff), min(256, down.shape[1])
    crow = per * cp
    half = crow // 2
    for chunk in range(NC):
        for s in range(chunk * per, (chunk + 1) * per):
            for q in tpeers:
                remote(arr.at[q, s], arr.at[q, s], sb.at[q, s], rb.at[q, s], ep, q).wait_recv()

        @pl.loop(0, ff // tile)
        def _(n):
            cols = pl.ds(pl.multiple_of(n * tile, tile), tile)
            g = jnp.zeros((crow, tile), F32)
            u = jnp.zeros((crow, tile), F32)
            for q in range(T):
                x = arr[q, chunk * per:(chunk + 1) * per].reshape(crow, width)
                g += dot(x, gate[q * width:(q + 1) * width, cols])
                u += dot(x, up[q * width:(q + 1) * width, cols])
            hidden[tp, chunk, :, cols] = (g / (1.0 + jnp.exp(-g)) * u).astype(BF16)

        for q in (xp, yp) if square else tpeers:
            c = remote(hidden.at[tp, chunk], hidden.at[tp, chunk], sh.at[q, chunk], rh.at[tp, chunk], ep, q)
            c.start()
            sends.append(c)

    for s in eps_back:
        remote(kv.at[s], kv.at[s], skv.at[s], rkv.at[s], s, tp).wait_recv()
        remote(rk.at[s], rk.at[s], srk.at[s], rrk.at[s], s, tp).wait_recv()
    raw = jnp.concatenate([rk[s].astype(F32) for s in range(E)], axis=1)
    front, back = raw[:ROT // 2], raw[ROT // 2:]
    key_rot = jnp.concatenate(
        [front * cosk[...] - back * sink[...], front * sink[...] + back * cosk[...]], axis=0
    )
    scale = (PLAIN + ROT) ** (-0.5)
    length = E * tokens
    heads_here = kw // PLAIN
    outs = []
    for h in range(heads_here):
        key = kv[:, :, h * PLAIN:(h + 1) * PLAIN].reshape(length, PLAIN)
        value = kv[:, :, kw + h * VALUE:kw + (h + 1) * VALUE].reshape(length, VALUE)
        scores = (
            dot_t(query[:, h * PLAIN:(h + 1) * PLAIN], key)
            + jnp.dot(
                query_rot[:, h * ROT:(h + 1) * ROT], key_rot,
                precision=lax.Precision.HIGHEST, preferred_element_type=F32,
            )
        ) * scale
        weights = jnp.exp(scores - jnp.max(scores, axis=-1, keepdims=True))
        total = jnp.sum(weights, axis=-1, keepdims=True)
        outs.append((dot(weights.astype(BF16), value) / total).astype(BF16))
    heads[tp] = jnp.concatenate(outs, axis=1)

    def relay(chunk):
        remote(hidden.at[yp, chunk], hidden.at[yp, chunk], sh.at[yp, chunk], rh.at[yp, chunk], ep, yp).wait_recv()
        c = remote(
            hidden.at[yp, chunk, pl.ds(0, half)], hidden.at[yp, chunk, pl.ds(0, half)],
            sd2.at[0, chunk], rd2.at[0, chunk], ep, xp,
        )
        c.start()
        sends.append(c)
        remote(hidden.at[xp, chunk], hidden.at[xp, chunk], sh.at[xp, chunk], rh.at[xp, chunk], ep, xp).wait_recv()
        c = remote(
            hidden.at[xp, chunk, pl.ds(half, half)], hidden.at[xp, chunk, pl.ds(half, half)],
            sd2.at[1, chunk], rd2.at[1, chunk], ep, yp,
        )
        c.start()
        sends.append(c)

    if square:
        for chunk in range(NC):
            relay(chunk)
    for q in tpeers:
        c = remote(heads.at[tp], heads.at[tp], shd.at[q], rhd.at[tp], ep, q)
        c.start()
        sends.append(c)

    l_down.wait()
    features = down.shape[1]
    for chunk in range(NC):
        if square:
            remote(
                hidden.at[dg, chunk, pl.ds(0, half)], hidden.at[dg, chunk, pl.ds(0, half)],
                sd2.at[0, chunk], rd2.at[0, chunk], ep, xp,
            ).wait_recv()
            remote(
                hidden.at[dg, chunk, pl.ds(half, half)], hidden.at[dg, chunk, pl.ds(half, half)],
                sd2.at[1, chunk], rd2.at[1, chunk], ep, yp,
            ).wait_recv()
        else:
            for q in tpeers:
                remote(hidden.at[q, chunk], hidden.at[q, chunk], sh.at[q, chunk], rh.at[q, chunk], ep, q).wait_recv()

        @pl.loop(0, features // out_tile)
        def _(n):
            cols = pl.ds(pl.multiple_of(n * out_tile, out_tile), out_tile)
            acc = jnp.zeros((crow, out_tile), F32)
            for q in range(T):
                acc += dot(hidden[q, chunk], down[q * ff:(q + 1) * ff, cols])
            rows_out[chunk * per:(chunk + 1) * per, :, cols] = acc.astype(BF16).reshape(per, cp, out_tile)

        for s in range(chunk * per, (chunk + 1) * per):
            @pl.when(ep != s)
            def _(s=s):
                remote(rows_out.at[s], returned.at[ep], sr.at[s], rr.at[ep], s, tp).start()

    returned[ep] = rows_out[ep]

    for q in tpeers:
        remote(heads.at[q], heads.at[q], shd.at[q], rhd.at[q], ep, q).wait_recv()
        remote(shared.at[q], shared.at[q], ssh.at[q], rsh.at[q], ep, q).wait_recv()
    l_ow.wait()
    hw = heads.shape[2]
    acc = dot(heads[0], ow[0:hw])
    for q in range(1, T):
        acc += dot(heads[q], ow[q * hw:(q + 1) * hw])
    attended[...] = acc.astype(BF16)
    l_sd.wait()
    sw = shared.shape[2]
    acc = dot(shared[0], sd[0:sw])
    for q in range(1, T):
        acc += dot(shared[q], sd[q * sw:(q + 1) * sw])

    for s in eps_back:
        remote(returned.at[s], returned.at[s], sr.at[s], rr.at[s], s, tp).wait_recv()
    back_rows = returned[...].reshape(slots, features)
    routed = jnp.zeros((tokens, features), F32)
    for k, pick in ((0, pick0), (1, pick1)):
        column = jnp.broadcast_to(rweight[k:k + 1, :], (tokens, tokens)).T[:, 0:1]
        routed += tdot(pick.astype(BF16), back_rows) * column
    combined[...] = (acc + routed).astype(BF16)

    for c in sends:
        c.wait_send()
    for s in eps:
        remote(rows_out.at[s], returned.at[ep], sr.at[s], rr.at[ep], s, tp).wait_send()


def per_device(
    E, T,
    compressed_query, compressed_key_value, rotary_key, query_norm_scale, context_norm_scale,
    query_plain_weight, query_rotary_weight, key_up_weight, value_up_weight, output_weight,
    mixture_input, mixture_gain, routes, route_weight, expert_gate, expert_up, expert_down,
    shared_gate, shared_up, shared_down,
):
    tokens = compressed_query.shape[0]
    heads_here = query_plain_weight.shape[1] // PLAIN
    length = tokens * E
    inverse = 1.0 / 10000.0 ** (jnp.arange(0, ROT, 2, dtype=F32) / ROT)
    mine = (lax.axis_index("ep") * tokens + jnp.arange(tokens, dtype=jnp.int32)).astype(F32)
    angles = mine[:, None] * inverse[None, :]
    c, s = jnp.cos(angles), jnp.sin(angles)
    cosq = jnp.tile(jnp.concatenate([c, c], axis=1), (1, heads_here))
    sinq = jnp.tile(jnp.concatenate([-s, s], axis=1), (1, heads_here))
    angles = inverse[:, None] * jnp.arange(length, dtype=jnp.int32).astype(F32)[None, :]
    cosk, sink = jnp.cos(angles), jnp.sin(angles)

    rows = mixture_input.shape[0]
    model = mixture_input.shape[1]
    capacity = rows * TOPK * 3 // (2 * E)
    cp = -(-capacity // 16) * 16
    NC = 2
    width = model // T
    ff = expert_gate.shape[2]
    features = expert_down.shape[2]
    weights = (
        query_plain_weight, query_rotary_weight, key_up_weight, value_up_weight, output_weight,
        expert_gate[0], expert_up[0], expert_down[0], shared_gate, shared_up, shared_down,
    )
    small = (
        compressed_query, compressed_key_value, rotary_key.T, query_norm_scale[None], context_norm_scale[None],
        mixture_input, mixture_gain[None], routes.T, route_weight.T, cosq, sinq, cosk, sink,
    )
    dma = pltpu.SemaphoreType.DMA
    kw = key_up_weight.shape[1]
    sw = shared_gate.shape[1]
    scratch = [pltpu.VMEM(w.shape, BF16) for w in weights] + [
        pltpu.VMEM((rows, model), BF16),
        pltpu.VMEM((E, cp, width), BF16),
        pltpu.VMEM((T, E, cp, width), BF16),
        pltpu.VMEM((E, tokens, 2 * kw), BF16),
        pltpu.VMEM((E, ROT, tokens), BF16),
        pltpu.VMEM((T, rows, sw), BF16),
        pltpu.VMEM((T, tokens, kw), BF16),
        pltpu.VMEM((T, NC, E // NC * cp, ff), BF16),
        pltpu.VMEM((E, cp, features), BF16),
        pltpu.VMEM((E, cp, features), BF16),
        dma((len(weights),)),
        dma((E,)), dma((E,)),
        dma((T, E)), dma((T, E)),
        dma((E,)), dma((E,)),
        dma((E,)), dma((E,)),
        dma((T,)), dma((T,)),
        dma((T,)), dma((T,)),
        dma((T, NC)), dma((T, NC)),
        dma((2, NC)), dma((2, NC)),
        dma((E,)), dma((E,)),
    ]
    vmem = pl.BlockSpec(memory_space=pltpu.VMEM)
    return pl.pallas_call(
        functools.partial(body, E, T, NC),
        out_shape=(
            jax.ShapeDtypeStruct((tokens, output_weight.shape[1]), BF16),
            jax.ShapeDtypeStruct((rows, features), BF16),
        ),
        in_specs=[vmem] * len(small) + [pl.BlockSpec(memory_space=pl.ANY)] * len(weights),
        out_specs=(vmem, vmem),
        scratch_shapes=scratch,
        compiler_params=pltpu.CompilerParams(
            collective_id=0, has_side_effects=True, vmem_limit_bytes=56 * 1024 * 1024
        ),
    )(*small, *weights)


def solution(mesh):
    row, col = P("ep", None), P(None, "tp")
    three = P("ep", None, "tp")
    in_specs = (
        row, row, row, P(), P(), col, col, col, col, col,
        row, P(), row, row, three, three, three, col, col, col,
    )
    return jax.shard_map(
        functools.partial(per_device, mesh.shape["ep"], mesh.shape["tp"]),
        mesh=mesh, in_specs=in_specs, out_specs=(P("ep", "tp"), P("ep", "tp")), check_vma=False,
    )
```

time: 155 us -> 75.7 us (0.49)
  Pallas kernels: 0 us -> 66.8 us
  waiting for transfers between devices: 55.7 us -> 0 us
  blocking collectives: 31.1 us -> 0 us
  matrix products: 24.2 us -> 0 us
  between operations: 14.4 us -> 0.68 us
  starting transfers between devices: 11.2 us -> 0 us
  other arithmetic: 8.67 us -> 1.11 us
  local copies, waits for them, and re-layouts: 9.52 us -> 5.9 us
    pallas_call x0 -> x1, Pallas kernels: none -> 66.8 us  [per_device(): pl.pallas_call(functools.partial(body, E, T, NC), out_shape=(jax.ShapeDty...]
    all_to_all x2 -> x0, waiting for transfers between devices: 46.2 us -> none  [the longest x1 45.2 us: per_device(): lax.all_to_all(outgoing, 'ep', split_axis=0, concat_axis=0, tiled=True)]
    all_gather x3 -> x0, blocking collectives: 31.1 us -> none  [the longest x1 12.8 us: per_device(): lax.all_gather(rotary_key, 'ep', axis=0, tiled=True)]
    dot_general x14 -> x0, matrix products: 24.2 us -> none  [the longest x1 5.67 us: per_device(): jnp.dot(all_hidden, expert_down[0], preferred_element_type=jnp.float32)]
    all_to_all x2 -> x0, starting transfers between devices: 11.1 us -> none  [the longest x1 6.49 us: per_device(): lax.all_to_all(outgoing, 'ep', split_axis=0, concat_axis=0, tiled=True)]
    all_gather x2 -> x0, waiting for transfers between devices: 9.52 us -> none  [the longest x1 9.5 us: per_device(): lax.all_gather(hidden, 'tp', axis=1, tiled=True)]
    gather x2 -> x0, local copies, waits for them, and re-layouts: 4.42 us -> none  [the longest x1 3.13 us: per_device(): outgoing = padded[owners].reshape(experts, capacity, model_width)]
    reduce_sum x7 -> x0, other arithmetic: 4.06 us -> none  [the longest x1 1.33 us: per_device(): jnp.mean(centred * centred, axis=-1, keepdims=True) + 1e-05]
  transfers between devices with their start and end apart: 4 -> 0, of which waited for: 3 -> 0; matrix products, arithmetic and copies ran while one was open for 14% -> 0% of each run, Pallas kernels for 0% -> 0%
where the time goes in v1:
time: 75.7 us; the launch traced here: 74.5 us
  Pallas kernels  66.8 us (88%)
  local copies, waits for them, and re-layouts  5.9 us (8%)
  other arithmetic  1.11 us (1%)
    pallas_call x1, Pallas kernels, per_device(): pl.pallas_call(functools.partial(body, E, T, NC), out_shape=(jax.ShapeDty...  66.8 us
    unnamed x2, local copies, waits for them, and re-layouts  3.14 us

profile of v1, /device:TPU:0, one launch (start us, length us, event | category | flops | bytes accessed | tf_op | source)
XLA Modules:
  0.0 74.5 jit_solution(9250028976658414340)
XLA Ops:
  0.7 1.3 %broadcast_in_dim.6.qscale = f32[1,1536]{1,0:T(1,128)} reshape(f32[1536]{0:T(1024)} %param.23) | data formatting | bytes 12288 | tf_op jit(solution)/shard_map/broadcast_in_dim | solution.py:343
  2.0 0.1 fusion
  2.1 0.7 copy.22.cosq
  2.9 0.7 copy.23.sinq
  3.6 1.0 %multiply_sine_fusion = (f32[16,1024]{1,0:T(8,128)}, f32[16,1024]{1,0:T(8,128)}) fusion(f32[1024]{0:T(1024)S(1)} %iota_convert_fusion, f32[16]{0:T(128)S(1)} %negate_power_fusion), kind=kLoop, calls=%fused_computation | loop fusion | flops 16384 | bytes 135232 | tf_op jit(solution)/shard_map/sin | solution.py:328
  4.5 66.8 %shard_map.203 = (bf16[128,512]{1,0:T(8,128)(2,1)}, bf16[128,512]{1,0:T(8,128)(2,1)}) custom-call(bf16[128,1536]{1,0:T(8,128)(2,1)} %cq.1, bf16[128,512]{1,0:T(8,128)(2,1)} %ckv.1, bf16[32,128]{1,0:T(8,128)(2,1)} %bitcast.15, f32[1,1536]{1,0:T(1,128)} %broadcast_in_dim.6.qscale, f32[1,512]{1,0:T(1,128)} %bitcast.17, bf16[128,2048]{1,0:T(8,128)(2,1)} %mx.1, ...), custom_call_target="tpu_custom_call" | custom-call | tf_op jit(solution)/shard_map/pallas_call | solution.py:372
  71.3 1.6 %copy.26 = bf16[128,512]{1,0:T(8,128)(2,1)} copy(bf16[128,512]{1,0:T(8,128)(2,1)} %get-tuple-element.11) | data formatting | bytes 262144
  72.9 1.6 %copy.27 = bf16[128,512]{1,0:T(8,128)(2,1)} copy(bf16[128,512]{1,0:T(8,128)(2,1)} %get-tuple-element.12) | data formatting | bytes 262144
  (6 shorter events, 0.0 us)
